TPU v7x, 512 devices: a whole 4x4x16 slice. The times are simulated.
512 devices in a mesh: sp: 64 (over z, y), tp: 8 (over x, core).
Axes of the slice: x: 4, y: 4, z: 16, core: 2. Of those that a mesh axis runs over, the one named last changes fastest.
Arguments:
- tokens: bfloat16 [8192, 4096], P('sp'), may hold values from -6 to 6
- norm_gain: bfloat16 [4096], replicated, may hold values from 0.099609375 to 1.8984375
- w_pool_in: bfloat16 [4096, 1024], P('sp', 'tp'), may hold values from -0.09375 to 0.09375
- w_x: bfloat16 [4096, 2048], P('sp', 'tp'), may hold values from -0.09375 to 0.09375
- w_z: bfloat16 [4096, 2048], P('sp', 'tp'), may hold values from -0.09375 to 0.09375
- w_b: bfloat16 [4096, 1024], P('sp', 'tp'), may hold values from -0.09375 to 0.09375
- w_c: bfloat16 [4096, 1024], P('sp', 'tp'), may hold values from -0.09375 to 0.09375
- w_dt: bfloat16 [4096, 2, 32], P(None, None, 'tp'), may hold values from -0.09375 to 0.09375
- conv_x: bfloat16 [3, 2048], P(None, 'tp'), may hold values from -3.5 to 3.5
- conv_b: bfloat16 [3, 1024], P(None, 'tp'), may hold values from -3.5 to 3.5
- output_map_taps: bfloat16 [3, 1024], P(None, 'tp'), may hold values from -3.5 to 3.5
- decay_log: float32 [2, 32], P(None, 'tp'), may hold values from -16 to 0
- leak: float32 [8192, 2, 32], P('sp', None, 'tp'), may hold values from 0 to 2
- init_state: float32 [2, 32, 64, 128], P(None, 'tp'), may hold values from -162.9174 to 162.9174
- head_gain: bfloat16 [2048], P('tp'), may hold values from 0.099609375 to 1.8984375
- w_out: bfloat16 [3072, 4096], P('sp', 'tp'), may hold values from -0.109375 to 0.109375
Outputs:
- mixed: bfloat16 [8192, 4096], P('sp', 'tp')
All inputs are finite; a program needn't handle non-finite values.
Results may differ from a plain program's by a relative error of at most 0.01.
Values may be sent and summed in bfloat16 or wider, within the bound.
A program may use at most 64 MiB of HBM per device.

v0:
```python
import jax
import jax.numpy as jnp
from jax import lax
from jax.sharding import Mesh
from jax.sharding import PartitionSpec as P

POOL_GW = 256
MIXER_HEAD_SIZE = 64
STATE = 128
BLOCK = 128
SP = ("sp_0", "sp_1")


epsilon = 1e-06
windows = (2, 4, 8, 16)
pool_reach = 8


def sent_together(arrays, axis, dim, along):
    widths = [a.shape[along] for a in arrays]
    both = jnp.concatenate(arrays, axis=along)
    whole = lax.all_gather(both, axis, axis=dim, tiled=True)
    return tuple(jnp.split(whole, [sum(widths[:k]) for k in range(1, len(widths))], axis=along))


def with_halo(cells, sides, width):
    for axis, dim in sides:
        count = lax.axis_size(axis)
        ends = count - 1
        head = lax.slice_in_dim(cells, 0, width, axis=dim)
        tail = lax.slice_in_dim(cells, cells.shape[dim] - width, cells.shape[dim], axis=dim)
        cells = jnp.concatenate(
            [
                lax.ppermute(tail, axis, [(i, (i + 1) % count) for i in range(ends)]),
                cells,
                lax.ppermute(head, axis, [((i + 1) % count, i) for i in range(ends)]),
            ],
            axis=dim,
        )
    return cells


def filled_with(value, identity):
    return jax.tree.map(
        lambda a, e: jnp.broadcast_to(jnp.asarray(e, a.dtype), a.shape), value, identity
    )


def prefix_by_axis(value, axes, combine, identity, reverse):
    before = start = filled_with(value, identity)
    so_far = value
    for axis in reversed(axes):
        length, mine = (lax.axis_size(axis), lax.axis_index(axis))
        pieces = jax.tree.map(
            lambda part, kind: lax.all_gather(part.astype(kind), axis),
            so_far,
            (jnp.bfloat16, jnp.bfloat16),
        )
        inside, so_far = (start, start)
        for k in reversed(range(length)) if reverse else range(length):
            passed = k > mine if reverse else k < mine
            so_far = combine(
                so_far, jax.tree.map(lambda part, own: part[k].astype(own.dtype), pieces, value)
            )
            inside = jax.tree.map(lambda new, old: jnp.where(passed, new, old), so_far, inside)
        before = combine(inside, before)
    return before


def laid_out(pieces, dim):
    pieces = jnp.moveaxis(pieces, 0, dim)
    shape = pieces.shape
    return pieces.reshape(*shape[:dim], shape[dim] * shape[dim + 1], *shape[dim + 2 :])


def gather_packed(arrays, axis, dims):
    line = jnp.concatenate([a.reshape(-1) for a in arrays])
    lines, at, outs = (lax.all_gather(line, axis), 0, [])
    for a, dim in zip(arrays, dims):
        pieces = lines[:, at : at + a.size].reshape(-1, *a.shape)
        outs.append(laid_out(pieces, dim))
        at += a.size
    return tuple(outs)


def whole_of(value, axes, dim):
    if not axes:
        return value
    nearer = lax.all_gather(value, axes[-1], axis=dim, tiled=True)
    return whole_of(nearer, axes[:-1], dim)


def rounded(value):
    return lax.optimization_barrier(value.astype(jnp.bfloat16))


def window_means(padded, first_pos, seq_total, channel_group):
    count_rows = padded.shape[0] - 2 * pool_reach
    prefix = jnp.concatenate(
        [jnp.zeros((1, padded.shape[1]), jnp.float32), jnp.cumsum(padded, axis=0)], axis=0
    )
    element_index = first_pos + jnp.arange(count_rows, dtype=jnp.int32)
    result = jnp.zeros((count_rows, padded.shape[1]), jnp.float32)
    for group_id, window in enumerate(windows):
        low_reach = window // 2
        high_reach = window - 1 - low_reach
        upper_sum = prefix[pool_reach + high_reach + 1 : pool_reach + high_reach + 1 + count_rows]
        lower_sum = prefix[pool_reach - low_reach : pool_reach - low_reach + count_rows]
        tallied_items = (
            jnp.minimum(element_index + high_reach, seq_total - 1)
            - jnp.maximum(element_index - low_reach, 0)
            + 1
        )
        means = (upper_sum - lower_sum) / tallied_items.astype(jnp.float32)[:, None]
        result = jnp.where(channel_group[None, :] == group_id, means, result)
    return result


def conv_silu(extended, conv_weight):
    weight = conv_weight.astype(jnp.float32)
    values = extended.astype(jnp.float32)
    summed = values[:-2] * weight[0] + values[1:-1] * weight[1] + values[2:] * weight[2]
    return jax.nn.silu(summed)


def ssd_block(state_in, inputs):
    x_blk, b_blk, c_blk, dt_blk, decay_blk = inputs
    block_length = x_blk.shape[0]
    cumul = jnp.cumsum(decay_blk, axis=0)
    scores = jnp.einsum("ign,kgn->gik", c_blk, b_blk, preferred_element_type=jnp.float32)
    index = jnp.arange(block_length)
    below = index[:, None] >= index[None, :]
    cumul_t = jnp.transpose(cumul, (1, 2, 0))
    gap_log = cumul_t[:, :, :, None] - cumul_t[:, :, None, :]
    decay_mat = jnp.exp(jnp.where(below, gap_log, -jnp.inf))
    dt_t = jnp.transpose(dt_blk, (1, 2, 0))
    mixing = (scores[:, None] * decay_mat * dt_t[:, :, None, :]).astype(jnp.bfloat16)
    inner = jnp.einsum("gjik,kgjp->igjp", mixing, x_blk, preferred_element_type=jnp.float32)
    carried = jnp.exp(cumul)[..., None] * jnp.einsum(
        "ign,gjpn->igjp", c_blk.astype(jnp.float32), state_in, precision=lax.Precision.HIGHEST
    )
    to_end = jnp.exp(cumul[-1:] - cumul) * dt_blk
    scaled_b = (to_end[..., None] * b_blk.astype(jnp.float32)[:, :, None, :]).astype(jnp.bfloat16)
    state_out = jnp.exp(cumul[-1])[..., None, None] * state_in + jnp.einsum(
        "kgjp,kgjn->gjpn", x_blk, scaled_b, preferred_element_type=jnp.float32
    )
    return (state_out, inner + carried)


def nearby_orientation(heads_x, b_groups, c_groups, step_dir, decay_dir):
    block_count = heads_x.shape[0] // BLOCK

    def to_blocks(values_in):
        return values_in.reshape((block_count, BLOCK) + values_in.shape[1:])

    zero_state = jnp.zeros(
        (heads_x.shape[1], heads_x.shape[2], heads_x.shape[3], b_groups.shape[2]), jnp.float32
    )
    final_state, outputs = lax.scan(
        ssd_block,
        zero_state,
        (
            to_blocks(heads_x),
            to_blocks(b_groups),
            to_blocks(c_groups),
            to_blocks(step_dir),
            to_blocks(decay_dir),
        ),
    )
    cumul_span = jnp.cumsum(decay_dir, axis=0)
    return (outputs.reshape(heads_x.shape), final_state, jnp.exp(cumul_span[-1]), cumul_span)


def combine_states(earlier, later):
    return (earlier[0] * later[0], earlier[1] * later[0][..., None, None] + later[1])


def including_element(local_out, c_groups, cumul_span, entry):
    return local_out + jnp.exp(cumul_span)[..., None] * jnp.einsum(
        "tgn,gjpn->tgjp", c_groups.astype(jnp.float32), entry, precision=lax.Precision.HIGHEST
    )


def per_device(
    tokens,
    norm_gain,
    w_pool_in,
    w_x,
    w_z,
    w_b,
    w_c,
    w_dt,
    conv_x,
    conv_b,
    output_map_taps,
    decay_log,
    leak,
    init_state,
    head_gain,
    w_out,
):
    tok_rows = tokens.shape[0]
    token_f = tokens.astype(jnp.float32)
    normed = (
        token_f
        * lax.rsqrt(jnp.mean(token_f * token_f, axis=1, keepdims=True) + epsilon)
        * norm_gain.astype(jnp.float32)
    ).astype(jnp.bfloat16)
    w_pieces = sent_together((w_pool_in, w_x, w_z, w_b, w_c), SP, 0, 1)
    columns = normed
    pool_sum, x_sum, z_sum, b_sum, c_sum = tuple(
        (jnp.dot(columns, w_piece, preferred_element_type=jnp.float32) for w_piece in w_pieces)
    )
    pool_in = pool_sum.astype(jnp.bfloat16)
    ssd_x = x_sum.astype(jnp.bfloat16)
    gate_z = z_sum.astype(jnp.bfloat16)
    ssd_b = b_sum.astype(jnp.bfloat16)
    ssd_c = c_sum.astype(jnp.bfloat16)
    head_count = w_x.shape[1] // MIXER_HEAD_SIZE
    group_count = w_b.shape[1] // STATE
    per_group = head_count // group_count
    dt_raw = jnp.dot(
        normed, w_dt.reshape(w_dt.shape[0], 2 * head_count), preferred_element_type=jnp.float32
    ).reshape(tok_rows, 2, head_count)
    pool_width = pool_in.shape[1]
    conv_in = jnp.concatenate([ssd_x, ssd_b, ssd_c], axis=1)
    extended = with_halo(jnp.concatenate([pool_in, conv_in], axis=1), ((SP, 0),), pool_reach)
    pool_ext = extended[:, :pool_width]
    conv_ext = extended[pool_reach - 1 : pool_reach + tok_rows + 1, pool_width:]
    channel_group = (
        lax.axis_index("tp") * pool_width + jnp.arange(pool_width, dtype=jnp.int32)
    ) // POOL_GW
    first_pos = lax.axis_index(SP) * tok_rows
    seq_total = tok_rows * lax.axis_size(SP)
    pooled = (
        window_means(pool_ext.astype(jnp.float32), first_pos, seq_total, channel_group)
        - pool_in.astype(jnp.float32)
    ).astype(jnp.bfloat16)
    conv_weight = jnp.concatenate([conv_x, conv_b, output_map_taps], axis=1)
    convolved = rounded(conv_silu(conv_ext, conv_weight))
    x_width = w_x.shape[1]
    b_width = w_b.shape[1]
    heads_x = convolved[:, :x_width].reshape(tok_rows, group_count, per_group, MIXER_HEAD_SIZE)
    b_groups = convolved[:, x_width : x_width + b_width].reshape(tok_rows, group_count, STATE)
    c_groups = convolved[:, x_width + b_width :].reshape(tok_rows, group_count, STATE)
    step_size = jax.nn.softplus(dt_raw)
    log_decay = -step_size * jnp.exp(decay_log)[None] - leak
    step_size = step_size.reshape(tok_rows, 2, group_count, per_group)
    log_decay = log_decay.reshape(tok_rows, 2, group_count, per_group)
    start = init_state.reshape(2, group_count, per_group, MIXER_HEAD_SIZE, STATE)
    fwd_out, fwd_state, fwd_decay, fwd_cumul = nearby_orientation(
        heads_x, b_groups, c_groups, step_size[:, 0], log_decay[:, 0]
    )
    flip_x = heads_x[::-1]
    flip_b = b_groups[::-1]
    flip_c = c_groups[::-1]
    bwd_out, bwd_state, bwd_decay, bwd_cumul = nearby_orientation(
        flip_x, flip_b, flip_c, step_size[::-1, 1], log_decay[::-1, 1]
    )
    identity = (jnp.ones_like(fwd_decay), jnp.zeros_like(fwd_state))
    fwd_prefix = prefix_by_axis((fwd_decay, fwd_state), SP, combine_states, identity, False)
    bwd_prefix = prefix_by_axis((bwd_decay, bwd_state), SP, combine_states, identity, True)
    fwd_entry = fwd_prefix[1] + fwd_prefix[0][..., None, None] * start[0]
    bwd_entry = bwd_prefix[1] + bwd_prefix[0][..., None, None] * start[1]
    forward = including_element(fwd_out, c_groups, fwd_cumul, fwd_entry)
    backward = including_element(bwd_out, flip_c, bwd_cumul, bwd_entry)[::-1]
    gated = (forward + backward).reshape(tok_rows, head_count, MIXER_HEAD_SIZE) * jax.nn.silu(
        gate_z.astype(jnp.float32)
    ).reshape(tok_rows, head_count, MIXER_HEAD_SIZE)
    head_norm = gated * lax.rsqrt(jnp.mean(gated * gated, axis=2, keepdims=True) + epsilon)
    ssd_y = (head_norm.reshape(tok_rows, x_width) * head_gain.astype(jnp.float32)).astype(
        jnp.bfloat16
    )
    pooled_all, ssd_all = gather_packed((pooled, ssd_y), "tp", (1, 1))
    joined = jnp.concatenate([pooled_all, ssd_all], axis=1)
    columns = joined
    mixed = jnp.dot(columns, whole_of(w_out, SP, 0), preferred_element_type=jnp.float32)
    return mixed.astype(jnp.bfloat16)


def solution(mesh):
    finer = Mesh(mesh.devices.reshape(16, 4, mesh.shape["tp"]), ("sp_0", "sp_1", "tp"))
    placed = (
        P(SP, None),
        P(),
        P(SP, "tp"),
        P(SP, "tp"),
        P(SP, "tp"),
        P(SP, "tp"),
        P(SP, "tp"),
        P(None, None, "tp"),
        P(None, "tp"),
        P(None, "tp"),
        P(None, "tp"),
        P(None, "tp"),
        P(SP, None, "tp"),
        P(None, "tp", None, None),
        P("tp"),
        P(SP, "tp"),
    )
    return jax.shard_map(
        per_device, mesh=finer, in_specs=placed, out_specs=P(SP, "tp"), check_vma=False
    )
```

profile of v0, /device:TPU:2, one launch (start us, length us, event | category | flops | bytes accessed | tf_op | source)
XLA Modules:
  0.0 422.9 jit_solution(10993320732463690518)
XLA Ops:
  6.5 0.8 constant_dynamic-update-slice_fusion.4
  7.4 0.8 constant_dynamic-update-slice_fusion.3
  8.1 0.8 constant_dynamic-update-slice_fusion.2
  8.9 0.7 constant_dynamic-update-slice_fusion.1
  9.6 0.7 constant_dynamic-update-slice_fusion
  12.4 0.9 reshape.2328
  13.3 1.5 fusion
  14.9 1.7 compare_select_fusion
  17.0 10.0 %all_gather.57 = bf16[4,1,4]{2,1,0:T(2,128)(2,1)S(1)} all-gather(bf16[1,1,4]{2,1,0:T(2,128)(2,1)S(1)} %get-tuple-element.55), channel_id=1, replica_groups=mesh['sp_0'=16,'sp_1'=4,'tp'=8] {'sp_1'}, dimensions={0}, use_global_device_ids=true | all-gather | bytes 40 | tf_op jit(solution)/shard_map/all_gather | solution.py:55
  27.3 141.3 %all-gather.8.cloned.1.call-done = bf16[4096,896]{1,0:T(8,128)(2,1)} async-done(((bf16[64,896]{1,0:T(8,128)(2,1)}), bf16[4096,896]{1,0:T(8,128)(2,1)}) %all-gather.8.cloned.1.call-update) | async-done | bytes 7340048 | tf_op jit(solution)/shard_map/all_gather | solution.py:22
  168.6 1.9 convolution_convert_fusion.3
  170.6 1.8 convolution_convert_fusion.1
  172.4 1.8 convolution_convert_fusion.2
  174.2 2.1 fusion.16
  176.3 2.4 collective-permute-start
  178.7 1.3 collective-permute-start.1
  180.0 4.2 collective-permute-done.1
  185.0 15.7 %all-gather.1 = bf16[16,64,128]{2,1,0:T(8,128)(2,1)S(1)} all-gather(bf16[4,64,128]{2,1,0:T(8,128)(2,1)S(1)} %fusion.26), channel_id=3, replica_groups=mesh['sp_0'=16,'sp_1'=4,'tp'=8] {'sp_1'}, dimensions={0}, use_global_device_ids=true | all-gather | bytes 327680 | tf_op jit(solution)/shard_map/all_gather | solution.py:55
  200.7 0.7 fusion.67
  201.8 10.2 %all_gather.52 = bf16[4,1,4]{2,1,0:T(2,128)(2,1)S(1)} all-gather(bf16[1,1,4]{2,1,0:T(2,128)(2,1)S(1)} %get-tuple-element.53), channel_id=1, replica_groups=mesh['sp_0'=16,'sp_1'=4,'tp'=8] {'sp_1'}, dimensions={0}, use_global_device_ids=true | all-gather | bytes 40 | tf_op jit(solution)/shard_map/all_gather | solution.py:55
  212.4 12.3 %all-gather = bf16[16,64,128]{2,1,0:T(8,128)(2,1)S(1)} all-gather(bf16[4,64,128]{2,1,0:T(8,128)(2,1)S(1)} %fusion.25), channel_id=2, replica_groups=mesh['sp_0'=16,'sp_1'=4,'tp'=8] {'sp_1'}, dimensions={0}, use_global_device_ids=true | all-gather | bytes 327680 | tf_op jit(solution)/shard_map/all_gather | solution.py:55
  224.7 0.7 fusion.45
  225.5 12.9 %all_gather.64 = bf16[192,512]{1,0:T(8,128)(2,1)} all-gather(bf16[48,512]{1,0:T(8,128)(2,1)S(1)} %copy-done.2), channel_id=1, replica_groups=mesh['sp_0'=16,'sp_1'=4,'tp'=8] {'sp_1'}, dimensions={0}, use_global_device_ids=true | all-gather | bytes 245760 | tf_op jit(solution)/shard_map/all_gather | solution.py:89
  238.7 27.0 %all_gather.58 = bf16[16,1,4]{2,1,0:T(2,128)(2,1)S(1)} all-gather(bf16[1,1,4]{2,1,0:T(2,128)(2,1)S(1)} %multiply_convert_fusion.10), channel_id=1, replica_groups=mesh['sp_0'=16,'sp_1'=4,'tp'=8] {'sp_0'}, dimensions={0}, use_global_device_ids=true | all-gather | bytes 136 | tf_op jit(solution)/shard_map/all_gather | solution.py:55
  265.7 27.0 %all_gather.53 = bf16[16,1,4]{2,1,0:T(2,128)(2,1)S(1)} all-gather(bf16[1,1,4]{2,1,0:T(2,128)(2,1)S(1)} %multiply_convert_fusion.11), channel_id=1, replica_groups=mesh['sp_0'=16,'sp_1'=4,'tp'=8] {'sp_0'}, dimensions={0}, use_global_device_ids=true | all-gather | bytes 136 | tf_op jit(solution)/shard_map/all_gather | solution.py:55
  292.8 2.1 divide_multiply_fusion
  296.7 1.9 fusion.15
  299.1 39.8 %all-gather.10.cloned.1.call-done = bf16[16,1,4,64,128]{4,3,2,1,0:T(8,128)(2,1)} async-done(((bf16[1,1,4,64,128]{4,3,2,1,0:T(8,128)(2,1)}), bf16[16,1,4,64,128]{4,3,2,1,0:T(8,128)(2,1)}) %all-gather.10.cloned.1.call-update) | async-done | bytes 1048592 | tf_op jit(solution)/shard_map/all_gather | solution.py:55
  338.8 1.9 fusion.13
  341.4 13.4 %all-gather.2 = bf16[393216]{0:T(1024)(128)(2,1)S(1)} all-gather(bf16[49152]{0:T(1024)(128)(2,1)S(1)} %pad_maximum_fusion.5), channel_id=4, replica_groups=mesh['sp_0'=16,'sp_1'=4,'tp'=8] {'tp'}, dimensions={0}, use_global_device_ids=true | all-gather | bytes 884736 | tf_op jit(solution)/shard_map/all_gather | solution.py:78
  355.3 57.9 %all-gather.14.cloned.1.call-done = bf16[3072,512]{1,0:T(8,128)(2,1)} async-done(((bf16[192,512]{1,0:T(8,128)(2,1)}), bf16[3072,512]{1,0:T(8,128)(2,1)}) %all-gather.14.cloned.1.call-update) | async-done | bytes 3145744 | tf_op jit(solution)/shard_map/all_gather | solution.py:89
  413.3 3.1 convolution_convert_fusion
  (116 shorter events, 8.1 us)
Async XLA Ops:
  6.5 162.1 %copy-start = (bf16[128,4096]{1,0:T(8,128)(2,1)S(1)}, bf16[128,4096]{1,0:T(8,128)(2,1)}, u32[]{:S(2)}) copy-start(bf16[128,4096]{1,0:T(8,128)(2,1)} %param.16) | copy-start | bytes 3145732
  6.5 10.0 %copy-start.3 = (f32[128,2,4]{0,2,1:T(4,128)S(1)}, f32[128,2,4]{0,2,1:T(4,128)}, u32[]{:S(2)}) copy-start(f32[128,2,4]{0,2,1:T(4,128)} %param.28) | copy-start | bytes 12292
  6.5 162.1 %all-gather.8.cloned.1.call-start = ((), (), s32[]{:S(2)}) async-start(), calls=%async_computation | async-start | bytes 7454720 | tf_op jit(solution)/shard_map/all_gather | solution.py:22
  10.3 0.6 copy-start.1
  11.0 285.7 %all-gather.12.cloned.1.call-start = ((), (), s32[]{:S(2)}) async-start(), calls=%async_computation.2 | async-start | bytes 1114112 | tf_op jit(solution)/shard_map/all_gather | solution.py:55
  174.1 5.8 %copy-start.4 = (bf16[3,256]{1,0:T(4,128)(2,1)S(1)}, bf16[3,256]{1,0:T(4,128)(2,1)}, u32[]{:S(2)}) copy-start(bf16[3,256]{1,0:T(4,128)(2,1)} %param.24) | copy-start | bytes 4612
  174.1 5.8 %copy-start.5 = (bf16[3,128]{1,0:T(4,128)(2,1)S(1)}, bf16[3,128]{1,0:T(4,128)(2,1)}, u32[]{:S(2)}) copy-start(bf16[3,128]{1,0:T(4,128)(2,1)} %param.26) | copy-start | bytes 2308
  174.2 5.8 %copy-start.6 = (bf16[3,128]{1,0:T(4,128)(2,1)S(1)}, bf16[3,128]{1,0:T(4,128)(2,1)}, u32[]{:S(2)}) copy-start(bf16[3,128]{1,0:T(4,128)(2,1)} %param.25) | copy-start | bytes 2308
  176.3 3.7 collective-permute-start
  178.7 5.6 %collective-permute-start.1 = (bf16[8,640]{1,0:T(8,128)(2,1)S(1)}, bf16[8,640]{1,0:T(8,128)(2,1)S(1)}, u32[]{:S(2)}, u32[]{:S(2)}) collective-permute-start(bf16[8,640]{1,0:T(8,128)(2,1)S(1)} %get-tuple-element.48), channel_id=1, source_target_pairs={{8,0},{16,8},{24,16},{32,24},{40,32},{48,40},{56,48},{64,56},{72,6... | collective-permute-start | bytes 30728 | tf_op jit(solution)/shard_map/ppermute | solution.py:36
  180.0 45.5 %copy-start.2 = (bf16[48,512]{1,0:T(8,128)(2,1)S(1)}, bf16[48,512]{1,0:T(8,128)(2,1)}, u32[]{:S(2)}) copy-start(bf16[48,512]{1,0:T(8,128)(2,1)} %param.31) | copy-start | bytes 147460
  184.3 54.3 %copy-start.8 = (bf16[256]{0:T(256)(128)(2,1)S(1)}, bf16[256]{0:T(256)(128)(2,1)}, u32[]{:S(2)}) copy-start(bf16[256]{0:T(256)(128)(2,1)} %param.30) | copy-start | bytes 1540
  201.5 137.3 %all-gather.10.cloned.1.call-start = ((), (), s32[]{:S(2)}) async-start(), calls=%async_computation.1 | async-start | bytes 1114112 | tf_op jit(solution)/shard_map/all_gather | solution.py:55
  225.5 187.8 %all-gather.14.cloned.1.call-start = ((), (), s32[]{:S(2)}) async-start(), calls=%async_computation.3 | async-start | bytes 3342336 | tf_op jit(solution)/shard_map/all_gather | solution.py:89
  295.0 1.8 copy-start.7
Sparse Core Ops, SparseCore 0:
  11.1 157.4 all-gather.7
  201.6 67.4 all-gather.11
  271.2 67.5 all-gather.9
  340.8 72.4 all-gather.13
where the time goes:
time: 424 us; the launch traced here: 423 us
  waiting for transfers between devices  243 us (57%)
  blocking collectives  128 us (30%)
  matrix products  20.2 us (5%)
  between operations  13.8 us (3%)
  local copies, waits for them, and re-layouts  8.38 us (2%)
  other arithmetic  5.19 us (1%)
    all_gather x1, waiting for transfers between devices, sent_together(): whole = lax.all_gather(both, axis, axis=dim, tiled=True)  141 us
    all_gather x6, blocking collectives, prefix_by_axis(): lax.all_gather(part.astype(kind), axis)  102 us
    all_gather x1, waiting for transfers between devices, whole_of(): nearer = lax.all_gather(value, axes[-1], axis=dim, tiled=True)  57.9 us
    all_gather x2, waiting for transfers between devices, prefix_by_axis(): lax.all_gather(part.astype(kind), axis)  39.8 us
    all_gather x1, blocking collectives, gather_packed(): lines, at, outs = (lax.all_gather(line, axis), 0, [])  13.4 us
    all_gather x1, blocking collectives, whole_of(): nearer = lax.all_gather(value, axes[-1], axis=dim, tiled=True)  12.9 us
    dot_general x5, matrix products, per_device(): jnp.dot(columns, w_piece, preferred_element_type=jnp.float32)  9.64 us
  transfers between devices with their start and end apart: 6, of which 4 were waited for; matrix products, arithmetic and copies ran while one was open for 4% of the time, Pallas kernels for 0%

commit v1 on v0

v1 whole, which is shorter than its diff:
```python
import functools

import jax
import jax.numpy as jnp
from jax import lax
from jax.experimental import pallas as pl
from jax.experimental.pallas import tpu as pltpu
from jax.sharding import Mesh
from jax.sharding import PartitionSpec as P

MESH = pl.DeviceIdType.MESH
F32 = jnp.float32
BF16 = jnp.bfloat16

POOL_GW = 256
HEAD = 64
BLOCK = 128
EDGE = 16
EPS = 1e-06
PIECES = 4
CHUNKS = 4


def silu(v):
    return v / (1.0 + jnp.exp(-v))


def dot_t(a, b, precision=None):
    return lax.dot_general(
        a, b, (((1,), (1,)), ((), ())), precision=precision, preferred_element_type=F32
    )


def split3(v):
    hi = v.astype(BF16).astype(F32)
    mid = (v - hi).astype(BF16).astype(F32)
    lo = (v - hi - mid).astype(BF16).astype(F32)
    return hi, mid, lo


def decay_tile(fwd, bwd):
    row = lax.broadcasted_iota(jnp.int32, (16, 128), 0)
    tile = jnp.zeros((16, 128), F32)
    for k, part in enumerate(split3(fwd) + split3(bwd)):
        tile = jnp.where(row == k, jnp.broadcast_to(part, (16, 128)), tile)
    return tile.astype(BF16)


def decays_of(tile):
    t = tile.astype(F32)
    return t[0:1] + t[1:2] + t[2:3], t[3:4] + t[4:5] + t[5:6]


def kernel(
    dims,
    tok_hbm, gain, wp, wx, wz, wb, wc, wdt, cx, cb, cc, alog, leak, init, hgain, wo,
    out,
    tokv, normed, tsend, tall, wall, oall,
    r1s, r1r, r1o, r2s, r2r, r2o, conv, initv,
    us, ur, vs, vr, hs, hr, ds, dr, es, er,
    yin, heads, pmine, smine, joined,
    lsem, wss, wrs, oss, ors, tss, trs, hls, hlr,
    r1ss, r1rs, r2ss, r2rs, uss, urs, vss, vrs, hss, hrs, dss, drs, ess, ers,
    pss, prs, sss, srs, bss, brs,
):
    nz, ny, nx, nc = dims
    nq = 4
    nzh = nz // nq
    half = nz // 2
    ntp = nx * nc
    d_model = tok_hbm.shape[1]
    kq = d_model // ny
    wr = wp.shape[0]
    orow = wo.shape[0]
    z = lax.axis_index("z")
    y = lax.axis_index("y")
    xi = lax.axis_index("x")
    ci = lax.axis_index("c")
    t = xi * nc + ci
    zl = lax.rem(z, nq)
    zh = lax.div(z, nq)
    up = lax.rem(z + 1, nz)
    down = lax.rem(z + nz - 1, nz)

    def ypeer(k):
        return lax.rem(y + k, ny)

    def remote(src, dst, ssem, rsem, dev):
        return pltpu.make_async_remote_copy(
            src_ref=src, dst_ref=dst, send_sem=ssem, recv_sem=rsem,
            device_id=dev, device_id_type=MESH,
        )

    wrows = pl.ds(pl.multiple_of(z * wr, wr), wr)
    locals_ = [
        pltpu.make_async_copy(wx, wall.at[wrows, pl.ds(0, 256)], lsem.at[0]),
        pltpu.make_async_copy(wb, wall.at[wrows, pl.ds(256, 128)], lsem.at[1]),
        pltpu.make_async_copy(wc, wall.at[wrows, pl.ds(384, 128)], lsem.at[2]),
        pltpu.make_async_copy(wz, wall.at[wrows, pl.ds(512, 256)], lsem.at[3]),
        pltpu.make_async_copy(wp, wall.at[wrows, pl.ds(768, 128)], lsem.at[4]),
        pltpu.make_async_copy(tok_hbm, tokv, lsem.at[5]),
        pltpu.make_async_copy(wo, oall.at[z, y], lsem.at[6]),
        pltpu.make_async_copy(init, initv, lsem.at[7]),
    ]
    for c in locals_:
        c.start()
    barrier = pltpu.get_barrier_semaphore()
    count = 0
    for dz in (0, 1, nz - 1):
        for k in range(ny):
            if dz == 0 and k == 0:
                continue
            pl.semaphore_signal(
                barrier, inc=1, device_id={"z": lax.rem(z + dz, nz), "y": ypeer(k)}, device_id_type=MESH
            )
            count += 1

    def tp_dev(d):
        p = lax.rem(t + d, ntp)
        return {"x": lax.div(p, nc), "c": lax.rem(p, nc)}

    for d in range(1, ntp):
        pl.semaphore_signal(barrier, inc=1, device_id=tp_dev(d), device_id_type=MESH)
        count += 1
    for c in locals_[:5]:
        c.wait()
    pl.semaphore_wait(barrier, count)

    def ring_copy(k, way, p, sending):
        shift = k if sending else k + 1
        slot = lax.rem(z + nz - shift, nz) if way == 0 else lax.rem(z + shift, nz)
        rows = pl.ds(pl.multiple_of(slot * wr + (wr // PIECES) * p, wr // PIECES), wr // PIECES)
        return remote(
            wall.at[rows], wall.at[rows], wss.at[way, k, p], wrs.at[way, k, p],
            {"z": up if way == 0 else down},
        )

    def in_ring(k, way, p):
        return k < half - 1 or (way == 0) == (p < PIECES // 2)

    def ring_step(k):
        for p in range(PIECES):
            for way in (0, 1):
                if k > 0:
                    if not in_ring(k - 1, way, p):
                        continue
                    ring_copy(k - 1, way, p, False).wait_recv()
                if k < half and in_ring(k, way, p):
                    ring_copy(k, way, p, True).start()

    def oring_copy(k, way, sending):
        shift = k if sending else k + 1
        slot = lax.rem(z + nz - shift, nz) if way == 0 else lax.rem(z + shift, nz)
        return remote(
            oall.at[slot, y], oall.at[slot, y], oss.at[way, k], ors.at[way, k],
            {"z": up if way == 0 else down},
        )

    def in_oring(k, way):
        return k < half - 1 or way == 0

    def oring_step(k):
        for way in (0, 1):
            if k > 0:
                if not in_oring(k - 1, way):
                    continue
                oring_copy(k - 1, way, False).wait_recv()
            if k < half and in_oring(k, way):
                oring_copy(k, way, True).start()

    def bulk_copy(k, c, sending):
        col = y if sending else lax.rem(y + ny - k, ny)
        span = pl.ds(c * (nz // CHUNKS), nz // CHUNKS)
        return remote(
            oall.at[span, col], oall.at[span, col], bss.at[k - 1, c], brs.at[k - 1, c],
            {"y": ypeer(k)},
        )

    ring_step(0)

    locals_[5].wait()
    lane = lax.broadcasted_iota(jnp.int32, (16, 128), 1)

    def norm_rows(i, carry):
        rows = pl.ds(pl.multiple_of(16 * i, 16), 16)
        v = tokv[rows, :].astype(F32)
        ms = jnp.mean(v * v, axis=1, keepdims=True)
        n = (v * lax.rsqrt(ms + EPS) * gain[...].astype(F32)).astype(BF16)
        normed[rows, :] = n
        nf = n.astype(F32)
        for m in range(kq // 128):
            for h in range(ny // 2):
                a0 = wr * ny * (2 * m) + 128 * h
                a1 = wr * ny * (2 * m + 1) + 128 * h
                t0 = nf[:, a0 : a0 + 128]
                t1 = nf[:, a1 : a1 + 128]
                even = jnp.where(lane < 64, t0, pltpu.roll(t1, 64, 1))
                odd = jnp.where(lane < 64, pltpu.roll(t0, 64, 1), t1)
                tsend[2 * h, rows, 128 * m : 128 * m + 128] = even.astype(BF16)
                tsend[2 * h + 1, rows, 128 * m : 128 * m + 128] = odd.astype(BF16)
        return carry

    lax.fori_loop(0, 128 // 16, norm_rows, 0)

    def trows(src):
        return pl.ds(pl.multiple_of(EDGE + BLOCK * src, 16), BLOCK)

    def tok_copy(k, sending):
        src = y if sending else lax.rem(y + ny - k, ny)
        return remote(
            tsend.at[ypeer(k)], tall.at[trows(src)], tss.at[k - 1], trs.at[k - 1], {"y": ypeer(k)}
        )

    top = EDGE + BLOCK * ny

    def left_edge(k):
        return remote(
            tsend.at[k, pl.ds(BLOCK - EDGE, EDGE)], tall.at[pl.ds(0, EDGE)], hls.at[k], hlr.at[0],
            {"z": up, "y": k},
        )

    def right_edge(k):
        return remote(
            tsend.at[k, pl.ds(0, EDGE)], tall.at[pl.ds(top, EDGE)], hls.at[k], hlr.at[1],
            {"z": down, "y": k},
        )

    for k in (2, 1, 3):
        tok_copy(k, True).start()
    sends_left = jnp.logical_and(y == ny - 1, z < nz - 1)
    sends_right = jnp.logical_and(y == 0, z > 0)

    @pl.when(sends_left)
    def _():
        for k in range(ny):
            left_edge(k).start()

    @pl.when(sends_right)
    def _():
        for k in range(ny):
            right_edge(k).start()

    mine = pltpu.make_async_copy(tsend.at[y], tall.at[trows(y)], lsem.at[8])
    mine.start()

    @pl.when(z == 0)
    def _():
        tall[pl.ds(0, EDGE), :] = jnp.zeros((EDGE, kq), BF16)

    @pl.when(z == nz - 1)
    def _():
        tall[pl.ds(top, EDGE), :] = jnp.zeros((EDGE, kq), BF16)

    ring_step(1)
    dt = dot_t(wdt[...], normed[...])
    step = jnp.maximum(dt, 0.0) + jnp.log1p(jnp.exp(-jnp.abs(dt)))
    log_decay = -step * jnp.exp(alog[...]) - leak[...]
    ii = lax.broadcasted_iota(jnp.int32, (BLOCK, BLOCK), 0)
    jj = lax.broadcasted_iota(jnp.int32, (BLOCK, BLOCK), 1)
    low = ii >= jj
    upm = ii <= jj
    hp = lax.Precision.HIGHEST
    sum_f = jnp.dot(log_decay, upm.astype(F32), precision=hp, preferred_element_type=F32)
    sum_b = jnp.dot(log_decay, low.astype(F32), precision=hp, preferred_element_type=F32)
    row8 = lax.broadcasted_iota(jnp.int32, (8, BLOCK), 0)
    cum_t = jnp.where(row8 < 4, sum_f, sum_b)
    tot = jnp.where(
        row8 < 4,
        jnp.broadcast_to(sum_f[:, BLOCK - 1 : BLOCK], (8, BLOCK)),
        jnp.broadcast_to(sum_b[:, 0:1], (8, BLOCK)),
    )
    to_end_t = jnp.exp(tot - cum_t) * step
    stacked = jnp.concatenate([cum_t, to_end_t, jnp.zeros((112, BLOCK), F32)], axis=0)
    cols = jnp.transpose(stacked)

    for k in range(2, half):
        ring_step(k)
    locals_[6].wait()
    oring_step(0)
    ring_step(half)

    for k in (1, 2, 3):
        tok_copy(k, False).wait_recv()
    mine.wait()

    @pl.when(z > 0)
    def _():
        left_edge(0).wait_recv()

    @pl.when(z < nz - 1)
    def _():
        right_edge(0).wait_recv()

    ext = BLOCK + 2 * EDGE

    def part(k, lo, hi):
        rows = pl.ds(pl.multiple_of(BLOCK * ypeer(k), 16), ext)
        return jnp.dot(tall[rows, :], wall[:, lo:hi], preferred_element_type=F32)

    def r1_copy(k):
        return remote(r1s.at[k - 1], r1r.at[k - 1], r1ss.at[k - 1], r1rs.at[k - 1], {"y": ypeer(k)})

    def r2_copy(k):
        return remote(r2s.at[k - 1], r2r.at[k - 1], r2ss.at[k - 1], r2rs.at[k - 1], {"y": ypeer(k)})

    for k in (2, 1, 3):
        r1s[k - 1] = part(k, 0, 512).astype(BF16)
        r1_copy(k).start()
    for k in (2, 1, 3):
        r2s[k - 1] = part(k, 512, 896).astype(BF16)
        r2_copy(k).start()
    r1o[...] = part(0, 0, 512)
    r2o[...] = part(0, 512, 896)
    for k in range(1, 3):
        oring_step(k)

    for k in (1, 3, 2):
        r1_copy(k).wait_recv()
    total = r1o[...]
    for k in range(3):
        total = total + r1r[k].astype(F32)
    conv[...] = total.astype(BF16).astype(F32)
    taps = jnp.concatenate([cx[...], cb[...], cc[...]], axis=1).astype(F32)
    mixed = (
        conv[EDGE - 1 : EDGE - 1 + BLOCK, :] * taps[0:1]
        + conv[EDGE : EDGE + BLOCK, :] * taps[1:2]
        + conv[EDGE + 1 : EDGE + 1 + BLOCK, :] * taps[2:3]
    )
    cv = silu(mixed)
    xf = cv[:, 0:256].astype(BF16)
    bg = cv[:, 256:384].astype(BF16)
    cg = cv[:, 384:512].astype(BF16)
    bf = bg.astype(F32)
    xt = jnp.transpose(xf.astype(F32)).astype(BF16)

    def up_copy(k):
        return remote(us.at[ypeer(k)], ur.at[y], uss.at[k - 1], urs.at[k - 1], {"y": ypeer(k)})

    def up_recv(k):
        src = lax.rem(y + ny - k, ny)
        return remote(us.at[ypeer(k)], ur.at[src], uss.at[k - 1], urs.at[k - 1], {"y": ypeer(k)})

    for h in range(4):
        sb = jnp.concatenate(
            [(cols[:, 8 + h : 9 + h] * bf).astype(BF16), (cols[:, 12 + h : 13 + h] * bf).astype(BF16)], axis=1
        )
        st = jnp.dot(xt[64 * h : 64 * h + 64], sb, preferred_element_type=F32)
        us[h, 0:64, :] = st[:, 0:128].astype(BF16)
        us[h, 64:128, :] = st[:, 128:256].astype(BF16)
        us[h, 128:144, :] = decay_tile(tot[h : h + 1], tot[4 + h : 5 + h])
    for k in (2, 1, 3):
        up_copy(k).start()
    ur[pl.ds(y, 1)] = us[pl.ds(y, 1)]

    scores = dot_t(cg, bg)
    for h in range(4):
        gf = cols[:, h : h + 1] - cum_t[h : h + 1]
        gb = cols[:, 4 + h : 5 + h] - cum_t[4 + h : 5 + h]
        mf = scores * jnp.exp(jnp.where(low, gf, -jnp.inf)) * step[h : h + 1]
        mb = scores * jnp.exp(jnp.where(upm, gb, -jnp.inf)) * step[4 + h : 5 + h]
        mm = jnp.concatenate([mf.astype(BF16), mb.astype(BF16)], axis=1)
        xh = xf[:, 64 * h : 64 * h + 64]
        yin[:, 64 * h : 64 * h + 64] = jnp.dot(
            mm, jnp.concatenate([xh, xh], axis=0), preferred_element_type=F32
        )
    oring_step(3)

    for k in (1, 3, 2):
        up_recv(k).wait_recv()
    lf, lb = zip(*[decays_of(ur[j, 128:144, :]) for j in range(ny)])

    def totals(sf, sb, lf, lb):
        n = len(sf)
        gf, gb = sf[0], sb[n - 1]
        for j in range(1, n):
            gf = jnp.exp(lf[j]) * gf + sf[j]
            gb = jnp.exp(lb[n - 1 - j]) * gb + sb[n - 1 - j]
        return gf, gb, functools.reduce(lambda a, b: a + b, lf), functools.reduce(lambda a, b: a + b, lb)

    ysf = [ur[j, 0:64, :].astype(F32) for j in range(ny)]
    ysb = [ur[j, 64:128, :].astype(F32) for j in range(ny)]
    gf, gb, glf, glb = totals(ysf, ysb, lf, lb)
    tile = decay_tile(glf, glb)
    for q in range(nq):
        vs[q, 0:16, :] = gf[16 * q : 16 * q + 16].astype(BF16)
        vs[q, 16:32, :] = gb[16 * q : 16 * q + 16].astype(BF16)
        vs[q, 32:48, :] = tile

    def zq(k):
        return lax.rem(zl + k, nq)

    def v_copy(k, sending):
        src = zl if sending else lax.rem(zl + nq - k, nq)
        return remote(vs.at[zq(k)], vr.at[src], vss.at[k - 1], vrs.at[k - 1], {"z": zh * nq + zq(k)})

    for k in (2, 1, 3):
        v_copy(k, True).start()
    vr[pl.ds(zl, 1)] = vs[pl.ds(zl, 1)]
    oring_step(4)
    for k in (1, 3, 2):
        v_copy(k, False).wait_recv()
    zf, zb = zip(*[decays_of(vr[j, 32:48, :]) for j in range(nq)])
    zsf = [vr[j, 0:16, :].astype(F32) for j in range(nq)]
    zsb = [vr[j, 16:32, :].astype(F32) for j in range(nq)]
    hf, hb, hlf, hlb = totals(zsf, zsb, zf, zb)
    hs[0:16, :] = hf.astype(BF16)
    hs[16:32, :] = hb.astype(BF16)
    hs[32:48, :] = decay_tile(hlf, hlb)

    def h_copy(k, sending):
        src = zh if sending else lax.rem(zh + nzh - k, nzh)
        return remote(
            hs, hr.at[src], hss.at[k - 1], hrs.at[k - 1], {"z": lax.rem(zh + k, nzh) * nq + zl}
        )

    for k in range(1, nzh):
        h_copy(k, True).start()
    hr[pl.ds(zh, 1)] = hs[...].reshape(1, 48, 128)

    for k in (1, 3, 2):
        r2_copy(k).wait_recv()
    total = r2o[...]
    for k in range(3):
        total = total + r2r[k].astype(F32)
    pin = total[:, 256:384].astype(BF16).astype(F32)
    r2o[:, 0:256] = silu(total[:, 0:256].astype(BF16).astype(F32))

    def moved(v, by):
        return pltpu.roll(v, by % ext, 0)

    s2 = pin + moved(pin, 1)
    s4 = moved(s2, 1) + moved(s2, -1)
    s8 = moved(s4, 2) + moved(s4, -2)
    s16 = moved(s8, 4) + moved(s8, -4)
    group = lax.div(t * BLOCK, POOL_GW)
    lo_reach = lax.shift_left(jnp.int32(1), group)
    hi_reach = lo_reach - 1
    sums = jnp.where(group == 0, s2, jnp.where(group == 1, s4, jnp.where(group == 2, s8, s16)))
    first = (z * ny + y) * BLOCK
    pos = first + lax.broadcasted_iota(jnp.int32, (BLOCK, 128), 0)
    tally = jnp.minimum(pos + hi_reach, nz * ny * BLOCK - 1) - jnp.maximum(pos - lo_reach, 0) + 1
    own_rows = slice(EDGE, EDGE + BLOCK)
    pmine[...] = (sums[own_rows] / tally.astype(F32) - pin[own_rows]).astype(BF16)

    def p_copy(d, sending):
        src = t if sending else lax.rem(t + ntp - d, ntp)
        at = pl.ds(pl.multiple_of(128 * src, 128), 128)
        return remote(pmine, joined.at[:, at], pss.at[d - 1], prs.at[d - 1], tp_dev(d))

    def s_copy(d, sending):
        src = t if sending else lax.rem(t + ntp - d, ntp)
        at = pl.ds(pl.multiple_of(128 * ntp + 256 * src, 128), 256)
        return remote(smine, joined.at[:, at], sss.at[d - 1], srs.at[d - 1], tp_dev(d))

    for d in range(1, ntp):
        p_copy(d, True).start()
    joined[:, pl.ds(pl.multiple_of(128 * t, 128), 128)] = pmine[...]
    for k in range(5, half + 1):
        oring_step(k)
    for c in range(CHUNKS):
        for k in (2, 1, 3):
            bulk_copy(k, c, True).start()

    for k in range(1, nzh):
        h_copy(k, False).wait_recv()
    locals_[7].wait()
    quarter = pl.ds(pl.multiple_of(16 * zl, 16), 16)
    ef = initv[0, pl.ds(y, 1), quarter, :].reshape(16, 128)
    eb = initv[1, pl.ds(y, 1), quarter, :].reshape(16, 128)
    inf, inb = ef, eb
    hd = [decays_of(hr[j, 32:48, :]) for j in range(nzh)]
    for j in range(nzh):
        inf = jnp.where(zh == j, ef, inf)
        ef = jnp.exp(hd[j][0]) * ef + hr[j, 0:16, :].astype(F32)
        b = nzh - 1 - j
        inb = jnp.where(zh == b, eb, inb)
        eb = jnp.exp(hd[b][1]) * eb + hr[b, 16:32, :].astype(F32)
    for j in range(nq):
        ds[j, 0:16, :] = inf.astype(BF16)
        inf = jnp.exp(zf[j]) * inf + zsf[j]
        b = nq - 1 - j
        ds[b, 16:32, :] = inb.astype(BF16)
        inb = jnp.exp(zb[b]) * inb + zsb[b]

    def d_copy(k, sending):
        src = zl if sending else lax.rem(zl + nq - k, nq)
        return remote(ds.at[zq(k)], dr.at[src], dss.at[k - 1], drs.at[k - 1], {"z": zh * nq + zq(k)})

    for k in (2, 1, 3):
        d_copy(k, True).start()
    dr[pl.ds(zl, 1)] = ds[pl.ds(zl, 1)]
    for k in (1, 3, 2):
        d_copy(k, False).wait_recv()
    ef = jnp.concatenate([dr[q, 0:16, :] for q in range(nq)], axis=0).astype(F32)
    eb = jnp.concatenate([dr[q, 16:32, :] for q in range(nq)], axis=0).astype(F32)
    for j in range(ny):
        es[j, 0:64, :] = ef.astype(BF16)
        ef = jnp.exp(lf[j]) * ef + ysf[j]
        b = ny - 1 - j
        es[b, 64:128, :] = eb.astype(BF16)
        eb = jnp.exp(lb[b]) * eb + ysb[b]

    def e_copy(k, sending):
        src = y if sending else lax.rem(y + ny - k, ny)
        return remote(es.at[ypeer(k)], er.at[src], ess.at[k - 1], ers.at[k - 1], {"y": ypeer(k)})

    for k in (2, 1, 3):
        e_copy(k, True).start()
    er[pl.ds(y, 1)] = es[pl.ds(y, 1)]
    for k in (1, 3, 2):
        e_copy(k, False).wait_recv()

    for h in range(4):
        ch = dot_t(cg, er[h])
        v = (
            yin[:, 64 * h : 64 * h + 64]
            + jnp.exp(cols[:, h : h + 1]) * ch[:, 0:64]
            + jnp.exp(cols[:, 4 + h : 5 + h]) * ch[:, 64:128]
        )
        v = v * r2o[EDGE : EDGE + BLOCK, 64 * h : 64 * h + 64]
        v = v * lax.rsqrt(jnp.mean(v * v, axis=1, keepdims=True) + EPS)
        heads[:, 64 * h : 64 * h + 64] = v
    smine[...] = (heads[...] * hgain[...].astype(F32)).astype(BF16)
    for d in range(1, ntp):
        s_copy(d, True).start()
    joined[:, pl.ds(pl.multiple_of(128 * ntp + 256 * t, 128), 256)] = smine[...]
    for k in (1, 3, 2):
        for c in range(CHUNKS):
            bulk_copy(k, c, False).wait_recv()
    for d in range(1, ntp):
        p_copy(d, False).wait_recv()
    for d in range(1, ntp):
        s_copy(d, False).wait_recv()
    rows = ntp * 384
    acc = jnp.dot(
        joined[...], oall[...].reshape(rows, oall.shape[3]), preferred_element_type=F32
    )
    out[...] = acc.astype(BF16)

    for k in range(half):
        for way in (0, 1):
            for p in range(PIECES):
                if in_ring(k, way, p):
                    ring_copy(k, way, p, True).wait_send()
            if in_oring(k, way):
                oring_copy(k, way, True).wait_send()

    @pl.when(sends_left)
    def _():
        for k in range(ny):
            left_edge(k).wait_send()

    @pl.when(sends_right)
    def _():
        for k in range(ny):
            right_edge(k).wait_send()

    for k in (1, 2, 3):
        tok_copy(k, True).wait_send()
        r1_copy(k).wait_send()
        r2_copy(k).wait_send()
        up_copy(k).wait_send()
        v_copy(k, True).wait_send()
        d_copy(k, True).wait_send()
        e_copy(k, True).wait_send()
        for c in range(CHUNKS):
            bulk_copy(k, c, True).wait_send()
    for k in range(1, nzh):
        h_copy(k, True).wait_send()
    for d in range(1, ntp):
        p_copy(d, True).wait_send()
        s_copy(d, True).wait_send()


def per_device(
    dims,
    tokens, norm_gain, w_pool_in, w_x, w_z, w_b, w_c, w_dt, conv_x, conv_b, output_map_taps,
    decay_log, leak, init_state, head_gain, w_out,
):
    nz, ny, nx, nc = dims
    ntp = nx * nc
    d_model = tokens.shape[1]
    kq = d_model // ny
    half = nz // 2
    nzh = nz // 4
    ext = BLOCK + 2 * EDGE
    f_out = w_out.shape[1]
    wdt_t = jnp.transpose(w_dt, (1, 2, 0)).reshape(8, d_model)
    leak_t = jnp.transpose(leak, (1, 2, 0)).reshape(8, BLOCK)
    alog = decay_log.reshape(8, 1)
    any_ = pl.BlockSpec(memory_space=pl.ANY)
    vmem = pl.BlockSpec(memory_space=pltpu.VMEM)
    dma = pltpu.SemaphoreType.DMA

    def v(*shape, dtype=BF16):
        return pltpu.VMEM(shape, dtype)

    scratch = [
        v(BLOCK, d_model), v(BLOCK, d_model), v(ny, BLOCK, kq), v(BLOCK * ny + 2 * EDGE, kq),
        v(kq, 896), v(nz, ny, w_out.shape[0], f_out),
        v(3, ext, 512), v(3, ext, 512), v(ext, 512, dtype=F32),
        v(3, ext, 384), v(3, ext, 384), v(ext, 384, dtype=F32),
        v(ext, 512, dtype=F32), v(2, 4, 64, 128, dtype=F32),
        v(ny, 144, 128), v(ny, 144, 128), v(4, 48, 128), v(4, 48, 128), v(48, 128), v(nzh, 48, 128),
        v(4, 32, 128), v(4, 32, 128), v(ny, 128, 128), v(ny, 128, 128),
        v(BLOCK, 256, dtype=F32), v(BLOCK, 256, dtype=F32), v(BLOCK, 128), v(BLOCK, 256),
        v(BLOCK, 384 * ntp),
        dma((9,)), dma((2, half, PIECES)), dma((2, half, PIECES)), dma((2, half)), dma((2, half)),
        dma((3,)), dma((3,)), dma((ny,)), dma((2,)),
        dma((3,)), dma((3,)), dma((3,)), dma((3,)), dma((3,)), dma((3,)), dma((3,)), dma((3,)),
        dma((max(nzh - 1, 1),)), dma((max(nzh - 1, 1),)), dma((3,)), dma((3,)), dma((3,)), dma((3,)),
        dma((max(ntp - 1, 1),)), dma((max(ntp - 1, 1),)), dma((max(ntp - 1, 1),)), dma((max(ntp - 1, 1),)),
        dma((3, CHUNKS)), dma((3, CHUNKS)),
    ]
    return pl.pallas_call(
        functools.partial(kernel, dims),
        out_shape=jax.ShapeDtypeStruct((BLOCK, f_out), BF16),
        in_specs=[any_, vmem, any_, any_, any_, any_, any_, vmem, vmem, vmem, vmem, vmem, vmem, any_, vmem, any_],
        out_specs=vmem,
        scratch_shapes=scratch,
        compiler_params=pltpu.CompilerParams(
            collective_id=0, has_side_effects=True, vmem_limit_bytes=50 * 1024 * 1024
        ),
        name="layer",
    )(
        tokens, norm_gain.reshape(1, d_model), w_pool_in, w_x, w_z, w_b, w_c, wdt_t,
        conv_x, conv_b, output_map_taps, alog, leak_t, init_state, head_gain.reshape(1, 256), w_out,
    )


def build(devices, dims):
    finer = Mesh(devices.reshape(dims), ("z", "y", "x", "c"))
    sp, tp = ("z", "y"), ("x", "c")
    placed = (
        P(sp, None), P(), P(sp, tp), P(sp, tp), P(sp, tp), P(sp, tp), P(sp, tp), P(None, None, tp),
        P(None, tp), P(None, tp), P(None, tp), P(None, tp), P(sp, None, tp), P(None, tp, None, None),
        P(tp), P(sp, tp),
    )
    return jax.shard_map(
        functools.partial(per_device, dims), mesh=finer, in_specs=placed, out_specs=P(sp, tp), check_vma=False
    )


def solution(mesh):
    return build(mesh.devices, (16, 4, 4, 2))
```

time: 424 us -> 120 us (0.28)
  the two profiles are of different devices: /device:TPU:2 before, /device:TPU:9 now
where the time goes in v1:
time: 120 us
  Pallas kernels  112 us (93%)
  local copies, waits for them, and re-layouts  7.92 us (7%)
    pallas_call x1, Pallas kernels, per_device(): pl.pallas_call(functools.partial(kernel, dims), out_shape=jax.ShapeDtypeS...  112 us
    unnamed x27, local copies, waits for them, and re-layouts  5.55 us

profile of v1, /device:TPU:9, one launch (start us, length us, event | category | flops | bytes accessed | tf_op | source)
XLA Modules:
  0.0 119.7 jit_solution(5848136755433823553)
XLA Ops:
  0.0 0.0 copy-start.12
  0.0 0.0 copy-start.9
  0.0 0.0 copy-start.7
  0.0 0.6 copy-done.12
  0.7 0.8 reshape.20.alog
  1.4 0.0 copy-start.6
  1.4 0.7 reshape.15.gain
  2.1 0.0 copy-start.2
  2.2 0.0 copy-start.3
  2.2 0.0 copy-start.4
  2.2 0.0 copy-start.5
  2.2 0.9 reshape.16.wdt
  3.1 0.0 copy-done.9
  3.1 0.0 copy-done.7
  3.1 0.0 copy-done.6
  3.1 0.0 copy-done.2
  3.1 0.0 copy-done.3
  3.1 0.0 copy-done.4
  3.1 0.0 copy-done.5
  3.1 0.0 copy-start
  3.2 1.2 %copy-done = bf16[128,4096]{1,0:T(8,128)(2,1)S(1)} copy-done((bf16[128,4096]{1,0:T(8,128)(2,1)S(1)}, bf16[128,4096]{1,0:T(8,128)(2,1)}, u32[]{:S(2)}) %copy-start) | copy-done | bytes 1048600
  4.4 0.0 copy-start.1
  4.4 0.9 copy-done.1
  5.3 0.0 copy-start.8
  5.3 0.7 copy-done.8
  6.0 0.0 copy-start.10
  6.0 0.7 copy-done.10
  6.7 0.0 copy-start.11
  6.7 0.7 copy-done.11
  7.4 111.7 %layer.1 = bf16[128,512]{1,0:T(8,128)(2,1)S(1)} custom-call(bf16[128,4096]{1,0:T(8,128)(2,1)S(1)} %copy-done, bf16[1,4096]{1,0:T(2,128)(2,1)S(1)} %reshape.15.gain, bf16[64,128]{1,0:T(8,128)(2,1)S(1)} %copy-done.5, bf16[64,256]{1,0:T(8,128)(2,1)S(1)} %copy-done.3, bf16[64,256]{1,0:T(8,128)(2,1)S(1)} %copy-done.4, bf16[64,128]{1,0:T(8,128)(2,1)S(1)} %copy-done.6, ...), custom_call_target="tpu_custom_call" | custom-call | tf_op jit(solution)/shard_map/layer/pallas_call | solution.py:615
  119.1 0.7 copy.19
  (1 shorter events, 0.0 us)
Async XLA Ops:
  0.0 0.7 copy-start.12
  0.0 3.1 %copy-start.9 = (bf16[3,256]{1,0:T(4,128)(2,1)S(1)}, bf16[3,256]{1,0:T(4,128)(2,1)}, u32[]{:S(2)}) copy-start(bf16[3,256]{1,0:T(4,128)(2,1)} %cx.1) | copy-start | bytes 4612
  0.0 3.1 %copy-start.7 = (bf16[64,128]{1,0:T(8,128)(2,1)S(1)}, bf16[64,128]{1,0:T(8,128)(2,1)}, u32[]{:S(2)}) copy-start(bf16[64,128]{1,0:T(8,128)(2,1)} %wc.1) | copy-start | bytes 49156
  1.4 1.7 %copy-start.6 = (bf16[64,128]{1,0:T(8,128)(2,1)S(1)}, bf16[64,128]{1,0:T(8,128)(2,1)}, u32[]{:S(2)}) copy-start(bf16[64,128]{1,0:T(8,128)(2,1)} %wb.1) | copy-start | bytes 49156
  2.1 1.0 copy-start.2
  2.2 1.0 copy-start.3
  2.2 1.0 copy-start.4
  2.2 1.0 copy-start.5
  3.1 1.2 %copy-start = (bf16[128,4096]{1,0:T(8,128)(2,1)S(1)}, bf16[128,4096]{1,0:T(8,128)(2,1)}, u32[]{:S(2)}) copy-start(bf16[128,4096]{1,0:T(8,128)(2,1)} %tok_hbm.1) | copy-start | bytes 3145732
  4.4 0.9 copy-start.1
  5.3 0.7 copy-start.8
  6.0 0.7 copy-start.10
  6.7 0.7 copy-start.11
